TPU v7x, 256 devices: a whole 4x4x8 slice. The times are simulated.
256 devices in a mesh: dp: 4 (over y), kv: 32 (over z, x), tp: 2 (over core).
Axes of the slice: x: 4, y: 4, z: 8, core: 2. Of those that a mesh axis runs over, the one named last changes fastest.
Arguments:
- tokens: bfloat16 [16, 16, 2048], P('dp', None, 'kv'), may hold values from -6 to 6
- norm_gain: float32 [2048], P('kv'), may hold values from 0.1 to 1.9
- w_query: bfloat16 [2048, 1024], P('kv', 'tp'), may hold values from -0.125 to 0.125
- w_key: bfloat16 [2048, 1024], P('kv', 'tp'), may hold values from -0.125 to 0.125
- w_value: bfloat16 [2048, 1024], P('kv', 'tp'), may hold values from -0.125 to 0.125
- w_forget: bfloat16 [2048, 16], replicated, may hold values from -0.125 to 0.125
- forget_bias: float32 [16], replicated, may hold values from -2 to 4
- query_gain: float32 [64], replicated, may hold values from 0.1 to 1.9
- key_gain: float32 [64], replicated, may hold values from 0.1 to 1.9
- head_gain: float32 [64], replicated, may hold values from 0.1 to 1.9
- w_out: bfloat16 [1024, 2048], P('tp', 'kv'), may hold values from -0.1875 to 0.1875
- key_cache: bfloat16 [16, 16384, 1024], P('dp', 'kv', 'tp'), may hold values from -240 to 240
- value_cache: bfloat16 [16, 16384, 1024], P('dp', 'kv', 'tp'), may hold values from -6 to 6
- gate_cache: float32 [16, 16, 16384], P('dp', 'tp', 'kv'), may hold values from -1922 to 0, as said below
- lengths: int32 [16], P('dp'), may hold values from 15341 to 16364
- accepted: int32 [16], P('dp'), may hold values from 0 to 4
- parents: int32 [16, 16], P('dp'), may hold values from -1 to 14, as said below
Outputs:
- layer_out: bfloat16 [16, 16, 2048], P('dp', None, 'kv')
- new_keys: bfloat16 [16, 16384, 1024], P('dp', 'kv', 'tp')
- new_values: bfloat16 [16, 16384, 1024], P('dp', 'kv', 'tp')
- proposal_gates: float32 [16, 16, 16], P('dp', None, 'tp')
Inputs may be any that keep to these rules, and one draw needn't show every extreme that they name: `gate_cache`: each entry is the running sum of log forget gates up to its position, so entries never rise along positions; entries at and after lengths hold the last step's proposals in order. `parents`: proposal 0 follows the last accepted token (parent -1); every other proposal's parent is one of the three proposals before it.
All inputs are finite; a program needn't handle non-finite values.
Results may differ from a plain program's by a relative error of at most 0.0051.
The roundings to bfloat16 on the way count: a program that leaves them out, or rounds other values in their place, can miss the bound.
Values may be sent and summed in bfloat16 or wider, within the bound.
No kernel may reach another device: no remote copies, remote signals or barrier semaphores. Data moves between devices by JAX's collectives and lax.ppermute only.
A program may use at most 64 MiB of HBM per device.

v0:
```python
import jax
import jax.numpy as jnp
from jax import lax
from jax.sharding import PartitionSpec as P

EPSILON = 1e-06
MASKED = -1e30


def padded_to(lines, devices):
    spare = -lines.shape[0] % devices
    if not spare:
        return lines
    return jnp.concatenate([lines, jnp.zeros((spare, *lines.shape[1:]), lines.dtype)])


def from_everyone(array, axis):
    devices = lax.axis_size(axis)
    return lax.all_to_all(
        jnp.broadcast_to(array[None], (devices, *array.shape)), axis, 0, 0, tiled=True
    )


def joined_along(parts, dim):
    parts = jnp.moveaxis(parts, 0, dim)
    lengths = parts.shape
    return parts.reshape(*lengths[:dim], lengths[dim] * lengths[dim + 1], *lengths[dim + 2 :])


def collect(array, axis, dim):
    parts = from_everyone(array, axis)
    return joined_along(parts, dim)


def cut_along(array, dim, devices):
    before, after = (array.shape[:dim], array.shape[dim + 1 :])
    return jnp.moveaxis(array.reshape(*before, devices, -1, *after), dim, 0)


def summed_on_arrival(array, axis, dim):
    parts = cut_along(array, dim, lax.axis_size(axis))
    arrived = lax.all_to_all(parts, axis, split_axis=0, concat_axis=0, tiled=True)
    return arrived.sum(axis=0)


def total_of(array, axes):
    padded = padded_to(array, lax.axis_size(axes))
    whole = collect(summed_on_arrival(padded, axes, 0), axes, 0)
    return lax.slice_in_dim(whole, 0, len(array)).reshape(array.shape)


def packed_total(arrays, axis):
    ends = [0]
    for a in arrays:
        ends.append(ends[-1] + a.size)
    total = total_of(jnp.concatenate([a.ravel() for a in arrays]), axis)
    return tuple((total[b:e].reshape(a.shape) for a, b, e in zip(arrays, ends, ends[1:])))


def of_everyone(array, axis):
    return from_everyone(array, axis).astype(jnp.float32).sum(axis=0)


def head_norm(head_rows, gain_vec):
    mean_square = jnp.mean(head_rows * head_rows, axis=-1, keepdims=True)
    return head_rows * lax.rsqrt(mean_square + EPSILON) * gain_vec


def ancestry(parents):
    count_all = parents.shape[1]
    step_ids = jnp.arange(count_all, dtype=jnp.int32)
    step_matrix = (parents[:, :, None] == step_ids[None, None, :]).astype(jnp.float32)
    identity = jnp.broadcast_to(jnp.eye(count_all, dtype=jnp.float32), step_matrix.shape)

    def extend(turn_index, ancestors):
        return identity + jnp.einsum(
            "sij,sjk->sik", step_matrix, ancestors, precision=lax.Precision.HIGHEST
        )

    return lax.fori_loop(0, count_all, extend, identity)


def combine(earlier, later):
    earlier_max, earlier_total, earlier_sum = earlier
    later_max, later_total, later_sum = later
    row_max = jnp.maximum(earlier_max, later_max)
    earlier_scale = jnp.exp(earlier_max - row_max)
    later_scale = jnp.exp(later_max - row_max)
    spread = earlier_max.shape + (-1,)
    joined = (
        earlier_sum.reshape(spread) * earlier_scale[..., None]
        + later_sum.reshape(spread) * later_scale[..., None]
    )
    return (
        row_max,
        earlier_total * earlier_scale + later_total * later_scale,
        joined.reshape(earlier_sum.shape),
    )


def block_part(scores, live_mask, block_values):
    seq_count, heads_local, prop_count, key_count = scores.shape
    row_max = jnp.max(scores, axis=3)
    weights = jnp.where(live_mask, jnp.exp(scores - row_max[..., None]), 0.0)
    row_total = jnp.sum(weights, axis=3)
    weighted = jnp.einsum(
        "shpk,skhd->sphd",
        weights.astype(jnp.bfloat16),
        block_values,
        preferred_element_type=jnp.float32,
    )
    return (
        jnp.transpose(row_max, (0, 2, 1)),
        jnp.transpose(row_total, (0, 2, 1)),
        weighted.reshape(seq_count, prop_count, -1),
    )


def finish_rows(row_sums, inverse, query_gain, key_gain, heads_local):
    head_width = row_sums.shape[1] // 3
    head_size = head_width // heads_local
    row_count = row_sums.shape[0]
    raw_sums = row_sums * inverse[:, None]
    queries = head_norm(
        raw_sums[:, :head_width].reshape(row_count, heads_local, head_size), query_gain
    )
    keyed = head_norm(
        raw_sums[:, head_width : 2 * head_width].reshape(row_count, heads_local, head_size),
        key_gain,
    )
    return jnp.concatenate(
        [
            queries.reshape(row_count, head_width),
            keyed.reshape(row_count, head_width),
            raw_sums[:, 2 * head_width :],
        ],
        axis=1,
    ).astype(jnp.bfloat16)


def flatten_part(part_triple, rows_all):
    part_max, part_total, part_sum = part_triple
    return (
        part_max.reshape(rows_all, -1),
        part_total.reshape(rows_all, -1),
        part_sum.reshape(rows_all, -1),
    )


def shards(
    tokens,
    norm_gain,
    w_query,
    w_key,
    w_value,
    w_forget,
    forget_bias,
    query_gain,
    key_gain,
    head_gain,
    w_out,
    key_cache,
    value_cache,
    gate_cache,
    lengths,
    accepted,
    parents,
):
    seq_count, prop_count, width_in = tokens.shape
    pos_dev = key_cache.shape[1]
    heads_local = gate_cache.shape[1]
    head_width = key_cache.shape[2]
    head_size = head_width // heads_local
    rows_all = seq_count * prop_count
    full_width = w_forget.shape[0]
    kv_index = lax.axis_index("kv")
    tp_index = lax.axis_index("tp")
    flattened = tokens.reshape(rows_all, width_in).astype(jnp.float32)
    squares = jnp.sum(flattened * flattened, axis=1)
    scaled = (flattened * norm_gain).astype(jnp.bfloat16)
    w_rows = lax.dynamic_slice_in_dim(w_forget, kv_index * width_in, width_in, 0)
    gate_part = jnp.dot(scaled, w_rows, preferred_element_type=jnp.float32)
    w_joined = jnp.concatenate([w_query, w_key, w_value], axis=1)
    summed, gate_sum, square_sum = packed_total(
        (jnp.dot(scaled, w_joined, preferred_element_type=jnp.float32), gate_part, squares), "kv"
    )
    inverse = lax.rsqrt(square_sum / full_width + EPSILON)
    joined = finish_rows(summed, inverse, query_gain, key_gain, heads_local)
    log_all = jax.nn.log_sigmoid(gate_sum * inverse[:, None] + forget_bias)
    log_own = lax.dynamic_slice_in_dim(log_all, tp_index * heads_local, heads_local, 1)
    log_own = log_own.reshape(seq_count, prop_count, heads_local)
    queries = joined[:, :head_width].reshape(seq_count, prop_count, heads_local, head_size)
    keys_new = joined[:, head_width : 2 * head_width].reshape(
        seq_count, prop_count, heads_local, head_size
    )
    values_new = joined[:, 2 * head_width :].reshape(seq_count, prop_count, heads_local, head_size)
    ancestors = ancestry(parents)
    path_sum = jnp.einsum("sij,sjh->sih", ancestors, log_own, precision=lax.Precision.HIGHEST)
    base_pos = lengths + accepted
    positions = kv_index * pos_dev + jnp.arange(pos_dev, dtype=jnp.int32)
    score_scale = head_size ** (-0.5)
    cached_keys = key_cache.reshape(seq_count, pos_dev, heads_local, head_size)
    cached_values = value_cache.reshape(seq_count, pos_dev, heads_local, head_size)
    scores = jnp.einsum("sphd,skhd->shpk", queries, cached_keys, preferred_element_type=jnp.float32)
    scores = scores * score_scale - gate_cache[:, :, None, :]
    live_mask = (positions[None, :] < base_pos[:, None])[:, None, None, :]
    scores = jnp.where(live_mask, scores, MASKED)
    local_part = block_part(scores, live_mask, cached_values)
    hit_mask = positions[None, :] == (base_pos - 1)[:, None]
    boundary_local = jnp.sum(jnp.where(hit_mask[:, None, :], gate_cache, 0.0), axis=2)
    tree_live = (ancestors > 0.5)[:, None, :, :]
    owner_mask = jnp.any(hit_mask, axis=1)
    tree_scores = jnp.einsum(
        "sphd,sjhd->shpj", queries, keys_new, preferred_element_type=jnp.float32
    )
    tree_scores = (
        tree_scores * score_scale
        - jnp.transpose(path_sum, (0, 2, 1))[:, :, None, :]
        - boundary_local[:, :, None, None]
    )
    tree_scores = jnp.where(tree_live, tree_scores, MASKED)
    tree_max, tree_total, tree_sum = block_part(tree_scores, tree_live, values_new)
    tree_max = jnp.where(owner_mask[:, None, None], tree_max, MASKED)
    tree_total = jnp.where(owner_mask[:, None, None], tree_total, 0.0)
    tree_sum = jnp.where(owner_mask[:, None, None], tree_sum, 0.0)
    partial_value = combine(local_part, (tree_max, tree_total, tree_sum))
    flat_max, flat_total, flat_sum = flatten_part(partial_value, rows_all)
    got_max, got_total, got_sum = (
        lax.all_to_all(flat_max[None], "kv", split_axis=1, concat_axis=0, tiled=True),
        lax.all_to_all(flat_total[None], "kv", split_axis=1, concat_axis=0, tiled=True),
        lax.all_to_all(flat_sum[None], "kv", split_axis=1, concat_axis=0, tiled=True),
    )
    top = jnp.max(got_max, axis=0)
    factors = jnp.exp(got_max - top[None])
    own_rows = got_max.shape[1]
    summed_rows = jnp.sum(
        got_sum.reshape(got_sum.shape[0], own_rows, heads_local, head_size) * factors[..., None],
        axis=0,
    )
    merged = (top, jnp.sum(got_total * factors, axis=0), summed_rows.reshape(own_rows, head_width))
    row_max, row_total, weighted = merged
    attended = weighted.reshape(own_rows, heads_local, head_size) / row_total[..., None]
    own_normed = head_norm(attended, head_gain).astype(jnp.bfloat16).reshape(own_rows, head_width)
    normed = collect(own_normed, "kv", 0)
    out_term = jnp.dot(normed, w_out, preferred_element_type=jnp.float32)
    layer_out = (
        of_everyone(out_term.astype(jnp.bfloat16), "tp").astype(jnp.float32).astype(jnp.bfloat16)
    )
    layer_out = layer_out.reshape(seq_count, prop_count, -1)
    new_rows = jnp.concatenate(
        [
            keys_new.reshape(seq_count, prop_count, head_width),
            values_new.reshape(seq_count, prop_count, head_width),
        ],
        axis=2,
    )
    slot_index = positions[None, :, None] - base_pos[:, None, None]
    placing = slot_index == jnp.arange(prop_count, dtype=jnp.int32)[None, None, :]
    written = jnp.einsum(
        "skp,spc->skc", placing.astype(jnp.bfloat16), new_rows, preferred_element_type=jnp.float32
    ).astype(jnp.bfloat16)
    hit_rows = jnp.any(placing, axis=2)[..., None]
    new_keys = jnp.where(hit_rows, written[..., :head_width], key_cache)
    new_values = jnp.where(hit_rows, written[..., head_width:], value_cache)
    return (layer_out, new_keys, new_values, log_own)


def solution(mesh):
    placed = (
        P("dp", None, "kv"),
        P("kv"),
        P("kv", "tp"),
        P("kv", "tp"),
        P("kv", "tp"),
        P(),
        P(),
        P(),
        P(),
        P(),
        P("tp", "kv"),
        P("dp", "kv", "tp"),
        P("dp", "kv", "tp"),
        P("dp", "tp", "kv"),
        P("dp"),
        P("dp"),
        P("dp", None),
    )
    return jax.shard_map(
        shards,
        mesh=mesh,
        in_specs=placed,
        out_specs=(
            P("dp", None, "kv"),
            P("dp", "kv", "tp"),
            P("dp", "kv", "tp"),
            P("dp", None, "tp"),
        ),
        check_vma=False,
    )
```

profile of v0, /device:TPU:1, one launch (start us, length us, event | category | flops | bytes accessed | tf_op | source)
XLA Modules:
  0.0 130.6 jit_solution(2430243420172668842)
XLA Ops:
  0.7 0.8 multiply_reduce_fusion.2
  2.3 0.9 fusion.53
  3.3 1.1 fusion.23
  4.5 1.3 %all_to_all.43 = f32[32,1,3106]{2,1,0:T(1,128)} reshape(f32[99392]{0:T(1024)S(1)} %pad_maximum_fusion) | data formatting | bytes 795136 | tf_op jit(solution)/shard_map/all_to_all | solution.py:42
  5.8 11.9 %all-to-all-start = ((f32[32,1,3106]{2,1,0:T(1,128)}), f32[32,1,3106]{2,1,0:T(1,128)S(1)}, u32[]{:S(2)}, u32[]{:S(2)}) async-start(f32[32,1,3106]{2,1,0:T(1,128)} %all_to_all.43), calls=%async_computation | async-start | bytes 819200 | tf_op jit(solution)/shard_map/all_to_all | solution.py:42
  17.7 4.2 %while.11 = (s32[]{:T(128)}, f32[4,16,16]{2,1,0:T(8,128)S(1)}, s32[4,16]{1,0:T(4,128)S(1)}, f32[16,16]{1,0:T(8,128)S(1)}, s32[]{:T(128)}) while((s32[]{:T(128)}, f32[4,16,16]{2,1,0:T(8,128)S(1)}, s32[4,16]{1,0:T(4,128)S(1)}, f32[16,16]{1,0:T(8,128)S(1)}, s32[]{:T(128)}) %tuple.48), condition=%wide.region_6.7_spmd.clone, body=%wide.region_5.6_spmd.clone.sunk | while | flops 199682 | bytes 17725 | solution.py:80
  22.9 2.4 %copy.142 = bf16[4,512,512]{1,2,0:T(8,128)(2,1)} copy(bf16[4,512,512]{2,1,0:T(8,128)(2,1)S(1)} %copy-done.2) | data formatting | bytes 4194304 | tf_op args[11]
  25.3 2.8 %copy.144 = bf16[4,512,512]{1,2,0:T(8,128)(2,1)S(1)} copy(bf16[4,512,512]{2,1,0:T(8,128)(2,1)} %param.31) | data formatting | bytes 4194304 | tf_op args[12]
  28.1 3.5 %all-to-all-done = f32[32,1,3106]{2,1,0:T(1,128)S(1)} async-done(((f32[32,1,3106]{2,1,0:T(1,128)}), f32[32,1,3106]{2,1,0:T(1,128)S(1)}, u32[]{:S(2)}, u32[]{:S(2)}) %all-to-all-start) | async-done | bytes 397600 | tf_op jit(solution)/shard_map/all_to_all | solution.py:42
  31.9 1.0 broadcast_in_dim.148
  32.8 5.7 %all-to-all-start.1 = ((f32[32,1,3106]{2,1,0:T(1,128)}), f32[32,1,3106]{2,1,0:T(1,128)S(1)}, u32[]{:S(2)}, u32[]{:S(2)}) async-start(f32[32,1,3106]{2,1,0:T(1,128)} %broadcast_in_dim.148), calls=%async_computation.1 | async-start | bytes 819200 | tf_op jit(solution)/shard_map/all_to_all | solution.py:19
  39.3 1.3 fusion.64
  41.3 10.9 %all-to-all-done.1 = f32[32,1,3106]{2,1,0:T(1,128)S(1)} async-done(((f32[32,1,3106]{2,1,0:T(1,128)}), f32[32,1,3106]{2,1,0:T(1,128)S(1)}, u32[]{:S(2)}, u32[]{:S(2)}) %all-to-all-start.1) | async-done | bytes 397600 | tf_op jit(solution)/shard_map/all_to_all | solution.py:19
  52.1 1.0 reduce.4
  53.4 3.5 %slice.41 = f32[6212,16]{1,0:T(8,128)} reshape(f32[32,3106]{1,0:T(8,128)S(1)} %reduce.4) | data formatting | bytes 795136 | tf_op jit(solution)/shard_map/slice | solution.py:57
  60.6 2.1 %fusion.67 = (f32[4,8,16]{2,1,0:T(8,128)S(1)}, f32[4,8,16,512]{3,2,1,0:T(8,128)S(1)}) fusion(f32[4,8,512]{2,1,0:T(8,128)S(1)} %copy-done.7, bf16[4,512,8,64]{1,3,2,0:T(8,128)(2,1)} %bitcast.63, bf16[4,16,8,64]{3,2,1,0:T(8,128)(2,1)S(1)} %reshape.280, pred[4,512]{1,0:T(4,128)(4,1)S(1)} %copy-done.14), kind=kOutput, calls=%fused_computation.107 | convolution fusion | flops 34602496 | bytes 3280896 | tf_op jit(solution)/shard_map/sphd,skhd->shpk/dot_general | solution.py:204
  65.6 5.6 %all-to-all-start.4 = ((f32[1,64,8]{2,0,1:T(1,128)}), f32[1,64,8]{2,0,1:T(1,128)}, u32[]{:S(2)}, u32[]{:S(2)}) async-start(f32[1,64,8]{2,0,1:T(1,128)} %bitcast.13), calls=%async_computation.4 | async-start | bytes 65536 | tf_op jit(solution)/shard_map/all_to_all | solution.py:230
  71.2 1.4 %fusion.13 = f32[4,16,8,64]{3,1,2,0:T(8,128)S(1)} fusion(bf16[4,512,8,64]{1,3,2,0:T(8,128)(2,1)S(1)} %bitcast.62, f32[4,8,16,512]{3,2,1,0:T(8,128)S(1)} %get-tuple-element.96, f32[4,8,16]{2,1,0:T(8,128)S(1)} %get-tuple-element.95, pred[4,512]{1,0:T(4,128)(4,1)} %get-tuple-element.94, f32[4,16,8]{1,2,0:T(8,128)} %get-tuple-element.80), kind=kOutput, calls=%fused_computation.20 | convolution fusion | flops 34373632 | bytes 3282944 | tf_op jit(solution)/shard_map/shpk,skhd->sphd/dot_general | solution.py:106
  72.6 0.9 slice.73
  73.7 1.4 %copy.165 = f32[4,16,8]{2,1,0:T(8,128)} copy(f32[4,16,8]{1,2,0:T(8,128)} %get-tuple-element.81) | data formatting | bytes 4096 | tf_op jit(solution)/shard_map/broadcast_in_dim;reshape | solution.py:229
  75.1 4.7 %all-to-all-done.4 = f32[1,64,8]{2,0,1:T(1,128)} async-done(((f32[1,64,8]{2,0,1:T(1,128)}), f32[1,64,8]{2,0,1:T(1,128)}, u32[]{:S(2)}, u32[]{:S(2)}) %all-to-all-start.4) | async-done | bytes 2080 | tf_op jit(solution)/shard_map/all_to_all | solution.py:230
  79.8 4.4 %all-to-all-start.3 = ((f32[1,64,8]{2,0,1:T(1,128)}), f32[1,64,8]{2,0,1:T(1,128)S(1)}, u32[]{:S(2)}, u32[]{:S(2)}) async-start(f32[1,64,8]{2,0,1:T(1,128)} %bitcast.9), calls=%async_computation.3 | async-start | bytes 65536 | tf_op jit(solution)/shard_map/all_to_all | solution.py:229
  84.2 1.2 fusion.10
  85.6 0.8 broadcast_in_dim_reshape_reshape.4
  86.4 6.5 %all-to-all-done.3 = f32[1,64,8]{2,0,1:T(1,128)S(1)} async-done(((f32[1,64,8]{2,0,1:T(1,128)}), f32[1,64,8]{2,0,1:T(1,128)S(1)}, u32[]{:S(2)}, u32[]{:S(2)}) %all-to-all-start.3) | async-done | bytes 2080 | tf_op jit(solution)/shard_map/all_to_all | solution.py:229
  92.9 4.0 %all-to-all-start.2 = ((f32[1,64,512]{2,0,1:T(1,128)}), f32[1,64,512]{2,0,1:T(1,128)S(1)}, u32[]{:S(2)}, u32[]{:S(2)}) async-start(f32[1,64,512]{2,0,1:T(1,128)} %broadcast_in_dim_reshape_reshape.4), calls=%async_computation.2 | async-start | bytes 262144 | tf_op jit(solution)/shard_map/all_to_all | solution.py:231
  97.0 3.2 %convolution_convert_fusion = bf16[4,512,1024]{2,1,0:T(8,128)(2,1)} fusion(bf16[4,16,512]{2,1,0:T(8,128)(2,1)S(1)} %bitcast.65, bf16[4,16,512]{2,1,0:T(8,128)(2,1)S(1)} %bitcast.64, s32[4,512]{1,0:T(4,128)S(1)} %copy-done.12), kind=kOutput, calls=%fused_computation.6 | convolution fusion | flops 69500928 | bytes 4333568 | tf_op jit(solution)/shard_map/skp,spc->skc/dot_general | solution.py:259
  101.6 4.6 %all-to-all-done.2 = f32[1,64,512]{2,0,1:T(1,128)S(1)} async-done(((f32[1,64,512]{2,0,1:T(1,128)}), f32[1,64,512]{2,0,1:T(1,128)S(1)}, u32[]{:S(2)}, u32[]{:S(2)}) %all-to-all-start.2) | async-done | bytes 131104 | tf_op jit(solution)/shard_map/all_to_all | solution.py:231
  107.5 4.4 %all-to-all-start.5 = ((bf16[32,2,512]{2,1,0:T(2,128)(2,1)}), bf16[32,2,512]{2,1,0:T(2,128)(2,1)S(1)}, u32[]{:S(2)}, u32[]{:S(2)}) async-start(bf16[32,2,512]{2,1,0:T(2,128)(2,1)} %broadcast_in_dim.162), calls=%async_computation.5 | async-start | bytes 131072 | tf_op jit(solution)/shard_map/all_to_all | solution.py:19
  111.9 4.4 %slice_select_fusion = (bf16[4,512,512]{2,1,0:T(8,128)(2,1)}, bf16[4,512,512]{2,1,0:T(8,128)(2,1)}) fusion(bf16[4,512,512]{2,1,0:T(8,128)(2,1)S(1)} %copy-done.1, bf16[4,512,1024]{2,1,0:T(8,128)(2,1)} %convolution_convert_fusion, pred[4,512]{1,0:T(4,128)(4,1)S(1)} %copy-done.16, bf16[4,512,512]{2,1,0:T(8,128)(2,1)} %param.30), kind=kLoop, calls=%fused_computation.7 | loop fusion | flops 2097152 | bytes 12584960 | tf_op jit(solution)/shard_map/jit(_where)/select_n | solution.py:264
  117.1 3.7 %all-to-all-done.5 = bf16[32,2,512]{2,1,0:T(2,128)(2,1)S(1)} async-done(((bf16[32,2,512]{2,1,0:T(2,128)(2,1)}), bf16[32,2,512]{2,1,0:T(2,128)(2,1)S(1)}, u32[]{:S(2)}, u32[]{:S(2)}) %all-to-all-start.5) | async-done | bytes 65568 | tf_op jit(solution)/shard_map/all_to_all | solution.py:19
  121.0 8.8 %all_to_all.61 = bf16[2,2,2048]{2,1,0:T(2,128)(2,1)S(1)} all-to-all(bf16[2,2,2048]{2,1,0:T(2,128)(2,1)S(1)} %reshape.291), channel_id=1, replica_groups=mesh['dp'=4,'kv'=32,'tp'=2] {'tp'}, dimensions={0} | all-to-all | bytes 32768 | tf_op jit(solution)/shard_map/all_to_all | solution.py:19
  (157 shorter events, 18.4 us)
Async XLA Ops:
  0.6 120.1 %copy-start = (bf16[512,64]{0,1:T(8,128)(2,1)S(1)}, bf16[512,64]{0,1:T(8,128)(2,1)}, u32[]{:S(2)}) copy-start(bf16[512,64]{0,1:T(8,128)(2,1)} %param.29) | copy-start | bytes 196612
  0.6 17.1 %copy-start.13 = (s32[4,16]{1,0:T(4,128)S(1)}, s32[4,16]{1,0:T(4,128)}, u32[]{:S(2)}) copy-start(s32[4,16]{1,0:T(4,128)} %param.35) | copy-start | bytes 772
  4.4 17.6 %copy-start.20 = (f32[64]{0:T(128)S(1)}, f32[64]{0:T(128)}, u32[]{:S(2)}) copy-start(f32[64]{0:T(128)} %param.26) | copy-start | bytes 772
  4.4 17.7 %copy-start.21 = (f32[64]{0:T(128)S(1)}, f32[64]{0:T(128)}, u32[]{:S(2)}) copy-start(f32[64]{0:T(128)} %param.27) | copy-start | bytes 772
  4.4 17.7 %copy-start.22 = (f32[64]{0:T(128)S(1)}, f32[64]{0:T(128)}, u32[]{:S(2)}) copy-start(f32[64]{0:T(128)} %param.28) | copy-start | bytes 772
  4.4 18.5 %copy-start.2 = (bf16[4,512,512]{2,1,0:T(8,128)(2,1)S(1)}, bf16[4,512,512]{2,1,0:T(8,128)(2,1)}, u32[]{:S(2)}) copy-start(bf16[4,512,512]{2,1,0:T(8,128)(2,1)} %param.30) | copy-start | bytes 6291460
  5.8 25.8 %all-to-all-start = ((f32[32,1,3106]{2,1,0:T(1,128)}), f32[32,1,3106]{2,1,0:T(1,128)S(1)}, u32[]{:S(2)}, u32[]{:S(2)}) async-start(f32[32,1,3106]{2,1,0:T(1,128)} %all_to_all.43), calls=%async_computation | async-start | bytes 819200 | tf_op jit(solution)/shard_map/all_to_all | solution.py:42
  22.9 40.5 %copy-start.10 = (pred[4,16,16]{1,2,0:T(8,128)(4,1)}, pred[4,16,16]{1,2,0:T(8,128)(4,1)S(1)}, u32[]{:S(2)}) copy-start(pred[4,16,16]{1,2,0:T(8,128)(4,1)S(1)} %copy.145) | copy-start | bytes 3076
  25.3 2.8 %copy-start.23 = (s32[4]{0:T(128)S(1)}, s32[4]{0:T(128)}, u32[]{:S(2)}) copy-start(s32[4]{0:T(128)} %param.33) | copy-start | bytes 52
  25.3 2.8 %copy-start.24 = (s32[4]{0:T(128)S(1)}, s32[4]{0:T(128)}, u32[]{:S(2)}) copy-start(s32[4]{0:T(128)} %param.34) | copy-start | bytes 52
  25.3 15.3 %copy-start.7 = (f32[4,8,512]{2,1,0:T(8,128)S(1)}, f32[4,8,512]{2,1,0:T(8,128)}, u32[]{:S(2)}) copy-start(f32[4,8,512]{2,1,0:T(8,128)} %param.32) | copy-start | bytes 196612
  32.8 19.3 %all-to-all-start.1 = ((f32[32,1,3106]{2,1,0:T(1,128)}), f32[32,1,3106]{2,1,0:T(1,128)S(1)}, u32[]{:S(2)}, u32[]{:S(2)}) async-start(f32[32,1,3106]{2,1,0:T(1,128)} %broadcast_in_dim.148), calls=%async_computation.1 | async-start | bytes 819200 | tf_op jit(solution)/shard_map/all_to_all | solution.py:19
  38.7 14.7 %copy-start.11 = (s32[4,512]{1,0:T(4,128)}, s32[4,512]{1,0:T(4,128)S(1)}, u32[]{:S(2)}) copy-start(s32[4,512]{1,0:T(4,128)S(1)} %broadcast_subtract_fusion) | copy-start | bytes 24580
  57.1 1.6 %copy-start.3 = (f32[64,1536]{1,0:T(8,128)}, f32[64,1536]{1,0:T(8,128)S(1)}, u32[]{:S(2)}) copy-start(f32[64,1536]{1,0:T(8,128)S(1)} %broadcast_multiply_fusion) | copy-start | bytes 1179652
  57.1 2.3 %copy-start.19 = (f32[16]{0:T(128)S(1)}, f32[16]{0:T(128)}, u32[]{:S(2)}) copy-start(f32[16]{0:T(128)} %param.25) | copy-start | bytes 196
  57.1 3.5 %copy-start.14 = (pred[4,512]{1,0:T(4,128)(4,1)S(1)}, pred[4,512]{1,0:T(4,128)(4,1)}, u32[]{:S(2)}) copy-start(pred[4,512]{1,0:T(4,128)(4,1)} %get-tuple-element.94) | copy-start | bytes 6148
  60.4 2.7 %copy-start.5 = (f32[64,8]{1,0:T(8,128)}, f32[64,8]{1,0:T(8,128)S(1)}, u32[]{:S(2)}) copy-start(f32[64,8]{1,0:T(8,128)S(1)} %fusion.42) | copy-start | bytes 6148
  60.6 2.5 %copy-start.9 = (bf16[4,16,8,64]{3,2,1,0:T(8,128)(2,1)S(1)}, bf16[4,16,8,64]{3,2,1,0:T(8,128)(2,1)}, u32[]{:S(2)}) copy-start(bf16[4,16,8,64]{3,2,1,0:T(8,128)(2,1)} %reshape.283) | copy-start | bytes 196612
  60.6 2.5 %copy-start.18 = (f32[4,8]{1,0:T(4,128)S(1)}, f32[4,8]{1,0:T(4,128)}, u32[]{:S(2)}) copy-start(f32[4,8]{1,0:T(4,128)} %select_reduce_fusion) | copy-start | bytes 388
  60.6 3.5 %copy-start.17 = (pred[4]{0:T(512)(128)(4,1)S(1)}, pred[4]{0:T(512)(128)(4,1)}, u32[]{:S(2)}) copy-start(pred[4]{0:T(512)(128)(4,1)} %get-tuple-element.82) | copy-start | bytes 16
  63.4 0.7 copy-start.4
  63.4 7.8 %copy-start.8 = (f32[4,8,16]{2,1,0:T(8,128)}, f32[4,8,16]{2,1,0:T(8,128)S(1)}, u32[]{:S(2)}) copy-start(f32[4,8,16]{2,1,0:T(8,128)S(1)} %get-tuple-element.97) | copy-start | bytes 6148
  65.6 14.3 %all-to-all-start.4 = ((f32[1,64,8]{2,0,1:T(1,128)}), f32[1,64,8]{2,0,1:T(1,128)}, u32[]{:S(2)}, u32[]{:S(2)}) async-start(f32[1,64,8]{2,0,1:T(1,128)} %bitcast.13), calls=%async_computation.4 | async-start | bytes 65536 | tf_op jit(solution)/shard_map/all_to_all | solution.py:230
  72.6 24.4 %copy-start.12 = (s32[4,512]{1,0:T(4,128)S(1)}, s32[4,512]{1,0:T(4,128)}, u32[]{:S(2)}) copy-start(s32[4,512]{1,0:T(4,128)} %copy-done.11) | copy-start | bytes 24580
  79.8 13.1 %all-to-all-start.3 = ((f32[1,64,8]{2,0,1:T(1,128)}), f32[1,64,8]{2,0,1:T(1,128)S(1)}, u32[]{:S(2)}, u32[]{:S(2)}) async-start(f32[1,64,8]{2,0,1:T(1,128)} %bitcast.9), calls=%async_computation.3 | async-start | bytes 65536 | tf_op jit(solution)/shard_map/all_to_all | solution.py:229
  92.9 13.3 %all-to-all-start.2 = ((f32[1,64,512]{2,0,1:T(1,128)}), f32[1,64,512]{2,0,1:T(1,128)S(1)}, u32[]{:S(2)}, u32[]{:S(2)}) async-start(f32[1,64,512]{2,0,1:T(1,128)} %broadcast_in_dim_reshape_reshape.4), calls=%async_computation.2 | async-start | bytes 262144 | tf_op jit(solution)/shard_map/all_to_all | solution.py:231
  97.0 9.8 %copy-start.15 = (f32[512]{0:T(512)S(1)}, f32[512]{0:T(512)}, u32[]{:S(2)}) copy-start(f32[512]{0:T(512)} %mul.237) | copy-start | bytes 6148
  97.0 14.9 %copy-start.1 = (bf16[4,512,512]{2,1,0:T(8,128)(2,1)S(1)}, bf16[4,512,512]{2,1,0:T(8,128)(2,1)}, u32[]{:S(2)}) copy-start(bf16[4,512,512]{2,1,0:T(8,128)(2,1)} %param.31) | copy-start | bytes 6291460
  97.0 14.9 %copy-start.16 = (pred[4,512]{1,0:T(4,128)(4,1)S(1)}, pred[4,512]{1,0:T(4,128)(4,1)}, u32[]{:S(2)}) copy-start(pred[4,512]{1,0:T(4,128)(4,1)} %fusion.35) | copy-start | bytes 6148
  107.5 13.2 %all-to-all-start.5 = ((bf16[32,2,512]{2,1,0:T(2,128)(2,1)}), bf16[32,2,512]{2,1,0:T(2,128)(2,1)S(1)}, u32[]{:S(2)}, u32[]{:S(2)}) async-start(bf16[32,2,512]{2,1,0:T(2,128)(2,1)} %broadcast_in_dim.162), calls=%async_computation.5 | async-start | bytes 131072 | tf_op jit(solution)/shard_map/all_to_all | solution.py:19
  111.9 4.5 %copy-start.6 = (f32[64,8]{1,0:T(8,128)S(1)}, f32[64,8]{1,0:T(8,128)}, u32[]{:S(2)}) copy-start(f32[64,8]{1,0:T(8,128)} %copy-done.5) | copy-start | bytes 6148
where the time goes:
time: 132 us; the launch traced here: 131 us
  starting transfers between devices  36 us (27%)
  waiting for transfers between devices  34 us (26%)
  local copies, waits for them, and re-layouts  21.5 us (16%)
  other arithmetic  14.3 us (11%)
  matrix products  14.2 us (11%)
  blocking collectives  8.85 us (7%)
    all_to_all x2, waiting for transfers between devices, from_everyone(): lax.all_to_all(jnp.broadcast_to(array[None], (devices, *array.shape)), ax...  14.6 us
    all_to_all x1, starting transfers between devices, summed_on_arrival(): lax.all_to_all(parts, axis, split_axis=0, concat_axis=0, tiled=True)  11.9 us
    all_to_all x2, starting transfers between devices, from_everyone(): lax.all_to_all(jnp.broadcast_to(array[None], (devices, *array.shape)), ax...  10.1 us
    all_to_all x1, blocking collectives, from_everyone(): lax.all_to_all(jnp.broadcast_to(array[None], (devices, *array.shape)), ax...  8.85 us
    all_to_all x1, waiting for transfers between devices, shards(): lax.all_to_all(flat_max[None], 'kv', split_axis=1, concat_axis=0, tiled=T...  6.53 us
    unnamed x54, local copies, waits for them, and re-layouts  6.18 us
    all_to_all x1, starting transfers between devices, shards(): lax.all_to_all(flat_total[None], 'kv', split_axis=1, concat_axis=0, tiled...  5.57 us
    all_to_all x1, waiting for transfers between devices, shards(): lax.all_to_all(flat_total[None], 'kv', split_axis=1, concat_axis=0, tiled...  4.74 us
  transfers between devices with their start and end apart: 6, of which 6 were waited for; matrix products, arithmetic and copies ran while one was open for 22% of the time, Pallas kernels for 0%

commit v1 on v0

--- a/solution.py
+++ b/solution.py
@@ -5,6 +5,12 @@
 
 EPSILON = 1e-06
 MASKED = -1e30
+
+
+def stacked_exchange(value, name, split, join):
+    pieces = jnp.split(value, lax.axis_size(name), axis=split)
+    received = lax.all_to_all(jnp.stack(pieces), name, 0, 0)
+    return jnp.concatenate(received, axis=join)
 
 
 def padded_to(lines, devices):
@@ -226,7 +232,7 @@
     partial_value = combine(local_part, (tree_max, tree_total, tree_sum))
     flat_max, flat_total, flat_sum = flatten_part(partial_value, rows_all)
     got_max, got_total, got_sum = (
-        lax.all_to_all(flat_max[None], "kv", split_axis=1, concat_axis=0, tiled=True),
+        stacked_exchange(flat_max[None], "kv", 1, 0),
         lax.all_to_all(flat_total[None], "kv", split_axis=1, concat_axis=0, tiled=True),
         lax.all_to_all(flat_sum[None], "kv", split_axis=1, concat_axis=0, tiled=True),
     )

time: 132 us -> 152 us (1.15)
  local copies, waits for them, and re-layouts: 21.5 us -> 41.2 us
  starting transfers between devices: 36 us -> 40.8 us
  waiting for transfers between devices: 34 us -> 29.3 us
    split x0 -> x34, local copies, waits for them, and re-layouts: none -> 20.1 us  [stacked_exchange(): pieces = jnp.split(value, lax.axis_size(name), axis=split)]
    all_to_all x1, starting transfers between devices: 4.4 us -> 9.15 us  [stacked_exchange(): received = lax.all_to_all(jnp.stack(pieces), name, 0, 0)]
    all_to_all x1, waiting for transfers between devices: 4.74 us -> 0.01 us  [shards(): lax.all_to_all(flat_total[None], 'kv', split_axis=1, concat_axis=0, tiled...]
    unnamed x54 -> x151, local copies, waits for them, and re-layouts: 6.18 us -> 7.07 us
  transfers between devices with their start and end apart: 6 -> 6, of which waited for: 6 -> 5; matrix products, arithmetic and copies ran while one was open for 22% -> 32% of each run, Pallas kernels for 0% -> 0%
where the time goes in v1:
time: 152 us; the launch traced here: 151 us
  local copies, waits for them, and re-layouts  41.2 us (27%)
  starting transfers between devices  40.8 us (27%)
  waiting for transfers between devices  29.3 us (19%)
  other arithmetic  14.4 us (9%)
  matrix products  14.3 us (9%)
  blocking collectives  8.81 us (6%)
  between operations  1.89 us (1%)
    split x34, local copies, waits for them, and re-layouts, stacked_exchange(): pieces = jnp.split(value, lax.axis_size(name), axis=split)  20.1 us
    all_to_all x2, waiting for transfers between devices, from_everyone(): lax.all_to_all(jnp.broadcast_to(array[None], (devices, *array.shape)), ax...  14.5 us
    all_to_all x1, starting transfers between devices, summed_on_arrival(): lax.all_to_all(parts, axis, split_axis=0, concat_axis=0, tiled=True)  11.9 us
    all_to_all x2, starting transfers between devices, from_everyone(): lax.all_to_all(jnp.broadcast_to(array[None], (devices, *array.shape)), ax...  10.2 us
    all_to_all x1, starting transfers between devices, stacked_exchange(): received = lax.all_to_all(jnp.stack(pieces), name, 0, 0)  9.15 us
    all_to_all x1, blocking collectives, from_everyone(): lax.all_to_all(jnp.broadcast_to(array[None], (devices, *array.shape)), ax...  8.81 us
    unnamed x151, local copies, waits for them, and re-layouts  7.07 us
    all_to_all x1, waiting for transfers between devices, stacked_exchange(): received = lax.all_to_all(jnp.stack(pieces), name, 0, 0)  6.52 us
  transfers between devices with their start and end apart: 6, of which 5 were waited for; matrix products, arithmetic and copies ran while one was open for 32% of the time, Pallas kernels for 0%

profile of v1, /device:TPU:1, one launch (start us, length us, event | category | flops | bytes accessed | tf_op | source)
XLA Modules:
  0.0 151.1 jit_solution(8580714541217813342)
XLA Ops:
  0.7 0.8 multiply_reduce_fusion.2
  2.3 0.9 fusion.54
  3.3 1.1 fusion.23
  4.5 1.3 all_to_all.37
  5.8 11.9 %all-to-all-start = ((f32[32,1,3106]{2,1,0:T(1,128)}), f32[32,1,3106]{2,1,0:T(1,128)S(1)}, u32[]{:S(2)}, u32[]{:S(2)}) async-start(f32[32,1,3106]{2,1,0:T(1,128)} %all_to_all.37), calls=%async_computation | async-start | bytes 819200 | tf_op jit(solution)/shard_map/all_to_all | solution.py:48
  17.7 4.2 %while.11 = (s32[]{:T(128)}, f32[4,16,16]{2,1,0:T(8,128)S(1)}, s32[4,16]{1,0:T(4,128)S(1)}, f32[16,16]{1,0:T(8,128)S(1)}, s32[]{:T(128)}) while((s32[]{:T(128)}, f32[4,16,16]{2,1,0:T(8,128)S(1)}, s32[4,16]{1,0:T(4,128)S(1)}, f32[16,16]{1,0:T(8,128)S(1)}, s32[]{:T(128)}) %tuple.79), condition=%wide.region_6.7_spmd.clone, body=%wide.region_5.6_spmd.clone.sunk | while | flops 199682 | bytes 17725 | solution.py:86
  22.9 2.4 %copy.446 = bf16[4,512,512]{1,2,0:T(8,128)(2,1)} copy(bf16[4,512,512]{2,1,0:T(8,128)(2,1)S(1)} %copy-done.2) | data formatting | bytes 4194304 | tf_op args[11]
  25.3 2.8 %copy.448 = bf16[4,512,512]{1,2,0:T(8,128)(2,1)S(1)} copy(bf16[4,512,512]{2,1,0:T(8,128)(2,1)} %param.31) | data formatting | bytes 4194304 | tf_op args[12]
  28.1 3.5 %all-to-all-done = f32[32,1,3106]{2,1,0:T(1,128)S(1)} async-done(((f32[32,1,3106]{2,1,0:T(1,128)}), f32[32,1,3106]{2,1,0:T(1,128)S(1)}, u32[]{:S(2)}, u32[]{:S(2)}) %all-to-all-start) | async-done | bytes 397600 | tf_op jit(solution)/shard_map/all_to_all | solution.py:48
  31.9 1.0 broadcast_in_dim.148
  32.8 5.7 %all-to-all-start.1 = ((f32[32,1,3106]{2,1,0:T(1,128)}), f32[32,1,3106]{2,1,0:T(1,128)S(1)}, u32[]{:S(2)}, u32[]{:S(2)}) async-start(f32[32,1,3106]{2,1,0:T(1,128)} %broadcast_in_dim.148), calls=%async_computation.1 | async-start | bytes 819200 | tf_op jit(solution)/shard_map/all_to_all | solution.py:25
  39.3 1.4 fusion.66
  41.3 10.8 %all-to-all-done.1 = f32[32,1,3106]{2,1,0:T(1,128)S(1)} async-done(((f32[32,1,3106]{2,1,0:T(1,128)}), f32[32,1,3106]{2,1,0:T(1,128)S(1)}, u32[]{:S(2)}, u32[]{:S(2)}) %all-to-all-start.1) | async-done | bytes 397600 | tf_op jit(solution)/shard_map/all_to_all | solution.py:25
  52.2 1.0 reduce.5
  53.4 3.5 %slice.41 = f32[6212,16]{1,0:T(8,128)} reshape(f32[32,3106]{1,0:T(8,128)S(1)} %reduce.5) | data formatting | bytes 795136 | tf_op jit(solution)/shard_map/slice | solution.py:63
  59.4 0.8 fusion.67
  60.6 2.1 %fusion.71 = (f32[4,8,16]{2,1,0:T(8,128)S(1)}, f32[4,8,16,512]{3,2,1,0:T(8,128)S(1)}) fusion(f32[4,8,512]{2,1,0:T(8,128)S(1)} %copy-done.7, bf16[4,512,8,64]{1,3,2,0:T(8,128)(2,1)} %bitcast.132, bf16[4,16,8,64]{3,2,1,0:T(8,128)(2,1)S(1)} %reshape.283, pred[4,512]{1,0:T(4,128)(4,1)S(1)} %copy-done.16), kind=kOutput, calls=%fused_computation.142 | convolution fusion | flops 34602496 | bytes 3280896 | tf_op jit(solution)/shard_map/sphd,skhd->shpk/dot_general | solution.py:210
  65.2 5.6 %all-to-all-start.4 = ((f32[1,64,8]{2,0,1:T(1,128)}), f32[1,64,8]{2,0,1:T(1,128)}, u32[]{:S(2)}, u32[]{:S(2)}) async-start(f32[1,64,8]{2,0,1:T(1,128)} %bitcast.44), calls=%async_computation.4 | async-start | bytes 65536 | tf_op jit(solution)/shard_map/all_to_all | solution.py:236
  91.6 1.4 fusion.13
  94.3 0.9 slice.73
  95.4 9.2 %all-to-all-start.3 = ((f32[32,1,2,8]{3,2,1,0:T(2,128)}), f32[32,1,2,8]{3,2,1,0:T(2,128)S(1)}, u32[]{:S(2)}, u32[]{:S(2)}) async-start(f32[32,1,2,8]{3,2,1,0:T(2,128)} %copy-done.15), calls=%async_computation.3 | async-start | bytes 65536 | tf_op jit(solution)/shard_map/all_to_all | solution.py:12
  104.5 1.2 fusion.10
  105.9 0.8 broadcast_in_dim_reshape_reshape.4
  106.7 6.5 %all-to-all-done.3 = f32[32,1,2,8]{3,2,1,0:T(2,128)S(1)} async-done(((f32[32,1,2,8]{3,2,1,0:T(2,128)}), f32[32,1,2,8]{3,2,1,0:T(2,128)S(1)}, u32[]{:S(2)}, u32[]{:S(2)}) %all-to-all-start.3) | async-done | bytes 2080 | tf_op jit(solution)/shard_map/all_to_all | solution.py:12
  113.2 4.0 %all-to-all-start.2 = ((f32[1,64,512]{2,0,1:T(1,128)}), f32[1,64,512]{2,0,1:T(1,128)S(1)}, u32[]{:S(2)}, u32[]{:S(2)}) async-start(f32[1,64,512]{2,0,1:T(1,128)} %broadcast_in_dim_reshape_reshape.4), calls=%async_computation.2 | async-start | bytes 262144 | tf_op jit(solution)/shard_map/all_to_all | solution.py:237
  117.3 3.3 %convolution_convert_fusion = bf16[4,512,1024]{2,1,0:T(8,128)(2,1)} fusion(bf16[4,16,512]{2,1,0:T(8,128)(2,1)S(1)} %bitcast.134, bf16[4,16,512]{2,1,0:T(8,128)(2,1)S(1)} %bitcast.133, s32[4,512]{1,0:T(4,128)S(1)} %copy-done.12), kind=kOutput, calls=%fused_computation.6 | convolution fusion | flops 69500928 | bytes 4333568 | tf_op jit(solution)/shard_map/skp,spc->skc/dot_general | solution.py:265
  120.6 0.8 multiply_reduce_fusion.1
  121.9 4.8 %all-to-all-done.2 = f32[1,64,512]{2,0,1:T(1,128)S(1)} async-done(((f32[1,64,512]{2,0,1:T(1,128)}), f32[1,64,512]{2,0,1:T(1,128)S(1)}, u32[]{:S(2)}, u32[]{:S(2)}) %all-to-all-start.2) | async-done | bytes 131104 | tf_op jit(solution)/shard_map/all_to_all | solution.py:237
  128.0 4.4 %all-to-all-start.5 = ((bf16[32,2,512]{2,1,0:T(2,128)(2,1)}), bf16[32,2,512]{2,1,0:T(2,128)(2,1)S(1)}, u32[]{:S(2)}, u32[]{:S(2)}) async-start(bf16[32,2,512]{2,1,0:T(2,128)(2,1)} %broadcast_in_dim.162), calls=%async_computation.5 | async-start | bytes 131072 | tf_op jit(solution)/shard_map/all_to_all | solution.py:25
  132.4 4.4 %slice_select_fusion = (bf16[4,512,512]{2,1,0:T(8,128)(2,1)}, bf16[4,512,512]{2,1,0:T(8,128)(2,1)}) fusion(bf16[4,512,512]{2,1,0:T(8,128)(2,1)S(1)} %copy-done.1, bf16[4,512,1024]{2,1,0:T(8,128)(2,1)} %convolution_convert_fusion, pred[4,512]{1,0:T(4,128)(4,1)S(1)} %copy-done.18, bf16[4,512,512]{2,1,0:T(8,128)(2,1)} %param.30), kind=kLoop, calls=%fused_computation.7 | loop fusion | flops 2097152 | bytes 12584960 | tf_op jit(solution)/shard_map/jit(_where)/select_n | solution.py:270
  137.6 3.7 %all-to-all-done.5 = bf16[32,2,512]{2,1,0:T(2,128)(2,1)S(1)} async-done(((bf16[32,2,512]{2,1,0:T(2,128)(2,1)}), bf16[32,2,512]{2,1,0:T(2,128)(2,1)S(1)}, u32[]{:S(2)}, u32[]{:S(2)}) %all-to-all-start.5) | async-done | bytes 65568 | tf_op jit(solution)/shard_map/all_to_all | solution.py:25
  141.5 8.8 %all_to_all.54 = bf16[2,2,2048]{2,1,0:T(2,128)(2,1)S(1)} all-to-all(bf16[2,2,2048]{2,1,0:T(2,128)(2,1)S(1)} %reshape.295), channel_id=1, replica_groups=mesh['dp'=4,'kv'=32,'tp'=2] {'tp'}, dimensions={0} | all-to-all | bytes 32768 | tf_op jit(solution)/shard_map/all_to_all | solution.py:25
  (290 shorter events, 37.9 us)
Async XLA Ops:
  0.6 140.6 %copy-start = (bf16[512,64]{0,1:T(8,128)(2,1)S(1)}, bf16[512,64]{0,1:T(8,128)(2,1)}, u32[]{:S(2)}) copy-start(bf16[512,64]{0,1:T(8,128)(2,1)} %param.29) | copy-start | bytes 196612
  0.6 17.1 %copy-start.13 = (s32[4,16]{1,0:T(4,128)S(1)}, s32[4,16]{1,0:T(4,128)}, u32[]{:S(2)}) copy-start(s32[4,16]{1,0:T(4,128)} %param.35) | copy-start | bytes 772
  4.4 17.6 %copy-start.53 = (f32[64]{0:T(128)S(1)}, f32[64]{0:T(128)}, u32[]{:S(2)}) copy-start(f32[64]{0:T(128)} %param.26) | copy-start | bytes 772
  4.4 17.7 %copy-start.54 = (f32[64]{0:T(128)S(1)}, f32[64]{0:T(128)}, u32[]{:S(2)}) copy-start(f32[64]{0:T(128)} %param.27) | copy-start | bytes 772
  4.4 17.7 %copy-start.55 = (f32[64]{0:T(128)S(1)}, f32[64]{0:T(128)}, u32[]{:S(2)}) copy-start(f32[64]{0:T(128)} %param.28) | copy-start | bytes 772
  4.4 18.5 %copy-start.2 = (bf16[4,512,512]{2,1,0:T(8,128)(2,1)S(1)}, bf16[4,512,512]{2,1,0:T(8,128)(2,1)}, u32[]{:S(2)}) copy-start(bf16[4,512,512]{2,1,0:T(8,128)(2,1)} %param.30) | copy-start | bytes 6291460
  5.8 25.8 %all-to-all-start = ((f32[32,1,3106]{2,1,0:T(1,128)}), f32[32,1,3106]{2,1,0:T(1,128)S(1)}, u32[]{:S(2)}, u32[]{:S(2)}) async-start(f32[32,1,3106]{2,1,0:T(1,128)} %all_to_all.37), calls=%async_computation | async-start | bytes 819200 | tf_op jit(solution)/shard_map/all_to_all | solution.py:48
  22.9 40.5 %copy-start.10 = (pred[4,16,16]{1,2,0:T(8,128)(4,1)}, pred[4,16,16]{1,2,0:T(8,128)(4,1)S(1)}, u32[]{:S(2)}) copy-start(pred[4,16,16]{1,2,0:T(8,128)(4,1)S(1)} %copy.449) | copy-start | bytes 3076
  25.3 2.8 %copy-start.56 = (s32[4]{0:T(128)S(1)}, s32[4]{0:T(128)}, u32[]{:S(2)}) copy-start(s32[4]{0:T(128)} %param.33) | copy-start | bytes 52
  25.3 2.8 %copy-start.57 = (s32[4]{0:T(128)S(1)}, s32[4]{0:T(128)}, u32[]{:S(2)}) copy-start(s32[4]{0:T(128)} %param.34) | copy-start | bytes 52
  25.3 15.4 %copy-start.7 = (f32[4,8,512]{2,1,0:T(8,128)S(1)}, f32[4,8,512]{2,1,0:T(8,128)}, u32[]{:S(2)}) copy-start(f32[4,8,512]{2,1,0:T(8,128)} %param.32) | copy-start | bytes 196612
  32.8 19.3 %all-to-all-start.1 = ((f32[32,1,3106]{2,1,0:T(1,128)}), f32[32,1,3106]{2,1,0:T(1,128)S(1)}, u32[]{:S(2)}, u32[]{:S(2)}) async-start(f32[32,1,3106]{2,1,0:T(1,128)} %broadcast_in_dim.148), calls=%async_computation.1 | async-start | bytes 819200 | tf_op jit(solution)/shard_map/all_to_all | solution.py:25
  38.7 14.7 %copy-start.11 = (s32[4,512]{1,0:T(4,128)}, s32[4,512]{1,0:T(4,128)S(1)}, u32[]{:S(2)}) copy-start(s32[4,512]{1,0:T(4,128)S(1)} %broadcast_subtract_fusion) | copy-start | bytes 24580
  57.1 2.4 %copy-start.52 = (f32[16]{0:T(128)S(1)}, f32[16]{0:T(128)}, u32[]{:S(2)}) copy-start(f32[16]{0:T(128)} %param.25) | copy-start | bytes 196
  57.1 3.5 %copy-start.16 = (pred[4,512]{1,0:T(4,128)(4,1)S(1)}, pred[4,512]{1,0:T(4,128)(4,1)}, u32[]{:S(2)}) copy-start(pred[4,512]{1,0:T(4,128)(4,1)} %get-tuple-element.130) | copy-start | bytes 6148
  60.4 2.7 %copy-start.5 = (f32[64,8]{1,0:T(8,128)}, f32[64,8]{1,0:T(8,128)S(1)}, u32[]{:S(2)}) copy-start(f32[64,8]{1,0:T(8,128)S(1)} %fusion.42) | copy-start | bytes 6148
  60.6 2.5 %copy-start.9 = (bf16[4,16,8,64]{3,2,1,0:T(8,128)(2,1)S(1)}, bf16[4,16,8,64]{3,2,1,0:T(8,128)(2,1)}, u32[]{:S(2)}) copy-start(bf16[4,16,8,64]{3,2,1,0:T(8,128)(2,1)} %reshape.286) | copy-start | bytes 196612
  60.6 2.5 %copy-start.51 = (f32[4,8]{1,0:T(4,128)S(1)}, f32[4,8]{1,0:T(4,128)}, u32[]{:S(2)}) copy-start(f32[4,8]{1,0:T(4,128)} %select_reduce_fusion) | copy-start | bytes 388
  60.6 2.9 %copy-start.19 = (pred[4]{0:T(512)(128)(4,1)S(1)}, pred[4]{0:T(512)(128)(4,1)}, u32[]{:S(2)}) copy-start(pred[4]{0:T(512)(128)(4,1)} %get-tuple-element.86) | copy-start | bytes 16
  63.4 28.2 %copy-start.8 = (f32[4,8,16]{2,1,0:T(8,128)}, f32[4,8,16]{2,1,0:T(8,128)S(1)}, u32[]{:S(2)}) copy-start(f32[4,8,16]{2,1,0:T(8,128)S(1)} %get-tuple-element.133) | copy-start | bytes 6148
  65.2 30.2 %all-to-all-start.4 = ((f32[1,64,8]{2,0,1:T(1,128)}), f32[1,64,8]{2,0,1:T(1,128)}, u32[]{:S(2)}, u32[]{:S(2)}) async-start(f32[1,64,8]{2,0,1:T(1,128)} %bitcast.44), calls=%async_computation.4 | async-start | bytes 65536 | tf_op jit(solution)/shard_map/all_to_all | solution.py:236
  91.5 2.1 %copy-start.22 = (f32[1,2,8]{2,1,0:T(2,128)S(1)}, f32[1,2,8]{2,1,0:T(2,128)}, u32[]{:S(2)}) copy-start(f32[1,2,8]{2,1,0:T(2,128)} %copy.490) | copy-start | bytes 196
  91.5 2.1 %copy-start.21 = (f32[1,2,8]{2,1,0:T(2,128)S(1)}, f32[1,2,8]{2,1,0:T(2,128)}, u32[]{:S(2)}) copy-start(f32[1,2,8]{2,1,0:T(2,128)} %copy.491) | copy-start | bytes 196
  91.6 2.1 %copy-start.20 = (f32[1,2,8]{2,1,0:T(2,128)S(1)}, f32[1,2,8]{2,1,0:T(2,128)}, u32[]{:S(2)}) copy-start(f32[1,2,8]{2,1,0:T(2,128)} %copy.492) | copy-start | bytes 196
  93.0 24.3 %copy-start.12 = (s32[4,512]{1,0:T(4,128)S(1)}, s32[4,512]{1,0:T(4,128)}, u32[]{:S(2)}) copy-start(s32[4,512]{1,0:T(4,128)} %copy-done.11) | copy-start | bytes 24580
  95.4 17.9 %all-to-all-start.3 = ((f32[32,1,2,8]{3,2,1,0:T(2,128)}), f32[32,1,2,8]{3,2,1,0:T(2,128)S(1)}, u32[]{:S(2)}, u32[]{:S(2)}) async-start(f32[32,1,2,8]{3,2,1,0:T(2,128)} %copy-done.15), calls=%async_computation.3 | async-start | bytes 65536 | tf_op jit(solution)/shard_map/all_to_all | solution.py:12
  113.2 13.5 %all-to-all-start.2 = ((f32[1,64,512]{2,0,1:T(1,128)}), f32[1,64,512]{2,0,1:T(1,128)S(1)}, u32[]{:S(2)}, u32[]{:S(2)}) async-start(f32[1,64,512]{2,0,1:T(1,128)} %broadcast_in_dim_reshape_reshape.4), calls=%async_computation.2 | async-start | bytes 262144 | tf_op jit(solution)/shard_map/all_to_all | solution.py:237
  117.3 10.0 %copy-start.17 = (f32[512]{0:T(512)S(1)}, f32[512]{0:T(512)}, u32[]{:S(2)}) copy-start(f32[512]{0:T(512)} %mul.237) | copy-start | bytes 6148
  117.3 15.1 %copy-start.1 = (bf16[4,512,512]{2,1,0:T(8,128)(2,1)S(1)}, bf16[4,512,512]{2,1,0:T(8,128)(2,1)}, u32[]{:S(2)}) copy-start(bf16[4,512,512]{2,1,0:T(8,128)(2,1)} %param.31) | copy-start | bytes 6291460
  117.3 15.1 %copy-start.18 = (pred[4,512]{1,0:T(4,128)(4,1)S(1)}, pred[4,512]{1,0:T(4,128)(4,1)}, u32[]{:S(2)}) copy-start(pred[4,512]{1,0:T(4,128)(4,1)} %fusion.35) | copy-start | bytes 6148
  128.0 13.3 %all-to-all-start.5 = ((bf16[32,2,512]{2,1,0:T(2,128)(2,1)}), bf16[32,2,512]{2,1,0:T(2,128)(2,1)S(1)}, u32[]{:S(2)}, u32[]{:S(2)}) async-start(bf16[32,2,512]{2,1,0:T(2,128)(2,1)} %broadcast_in_dim.162), calls=%async_computation.5 | async-start | bytes 131072 | tf_op jit(solution)/shard_map/all_to_all | solution.py:25
  132.4 4.5 %copy-start.6 = (f32[64,8]{1,0:T(8,128)S(1)}, f32[64,8]{1,0:T(8,128)}, u32[]{:S(2)}) copy-start(f32[64,8]{1,0:T(8,128)} %copy-done.5) | copy-start | bytes 6148
  (32 other events, 59.1 us)
